TPU v7x, 512 devices: a whole 4x8x8 slice. The times are simulated.
512 devices in a mesh: sp: 32 (over z, x), tp: 16 (over y, core).
Axes of the slice: x: 4, y: 8, z: 8, core: 2. Of those that a mesh axis runs over, the one named last changes fastest.
Arguments:
- skip_stream_entering: bfloat16 [4096, 2048], P('sp', 'tp'), may hold values from -24 to 24
- unfiltered_channel_feed: bfloat16 [4096, 2048], P('sp', 'tp'), may hold values from -6 to 6
- unfiltered_state_entry: bfloat16 [4096, 2048], P('sp', 'tp'), may hold values from -6 to 6
- unfiltered_state_exit: bfloat16 [4096, 2048], P('sp', 'tp'), may hold values from -6 to 6
- final_valve_preactivation: bfloat16 [4096, 2048], P('sp', 'tp'), may hold values from -6 to 6
- increment_preactivation: float32 [2, 32, 4096], P(None, 'tp', 'sp'), may hold values from -8 to 8
- summed_attenuation_both_ways: float32 [2, 32, 4096], P(None, 'tp', 'sp'), may hold values from -0.7 to 0, as said below
- channel_fading_speed: float32 [2, 32], P(None, 'tp'), may hold values from 4.8828125e-05 to 0.03, as said below
- channel_feed_filter: float32 [5, 2048], P(None, 'tp'), may hold values from -2.5 to 2.5
- state_entry_filter: float32 [5, 2048], P(None, 'tp'), may hold values from -2.5 to 2.5
- state_exit_filter: float32 [5, 2048], P(None, 'tp'), may hold values from -2.5 to 2.5
- clustered_rescale_factor: float32 [2048], P('tp'), may hold values from 0.1 to 1.9
- final_projection_weights: bfloat16 [2048, 2048], P(None, 'tp'), may hold values from -0.125 to 0.125
- specialist_rescale_factor: float32 [2048], replicated, may hold values from 0.1 to 1.9
- item_specialist_couple: int32 [4096, 2], P('sp'), may hold values from 0 to 31, all different within a row; in each aligned block of 128 rows (0 to 127, 128 to 255, ...) at most 16 rows name the same one
- selected_cluster_likelihood: float32 [4096], P('sp'), may hold values from 0.3 to 1
- selected_twin_scores_raw: float32 [4096, 2], P('sp'), may hold values from -6 to 6
- specialist_gating_weights: bfloat16 [32, 2048, 4096], P('sp', None, 'tp'), may hold values from -0.125 to 0.125
- specialist_raising_weights: bfloat16 [32, 2048, 4096], P('sp', None, 'tp'), may hold values from -0.125 to 0.125
- specialist_lowering_weights: bfloat16 [32, 4096, 2048], P('sp', 'tp'), may hold values from -0.09375 to 0.09375
Outputs:
- layer_out: bfloat16 [4096, 2048], P('sp', 'tp')
Inputs may be any that keep to these rules, and one draw needn't show every extreme that they name: For every head, dt times channel_fading_speed at the rate of the draw sets how far a state is carried; summed_attenuation_both_ways holds a few sharp losses of state. `summed_attenuation_both_ways`: mostly zero. `item_specialist_couple`: the two experts of a row differ. Among the rows of one index of sp (aligned blocks of 128 rows) no expert is named by more than 16 rows, a bound that some expert reaches in some blocks.
All inputs are finite; a program needn't handle non-finite values.
Results may differ from a plain program's by a relative error of at most 0.0095.
Values may be sent and summed in bfloat16 or wider, within the bound.
No kernel may reach another device: no remote copies, remote signals or barrier semaphores. Data moves between devices by JAX's collectives and lax.ppermute only.
A program may use at most 64 MiB of HBM per device.

v0:
```python
import jax
import jax.numpy as jnp
from jax import lax
from jax.sharding import Mesh
from jax.sharding import PartitionSpec as P

D = 2048
HD = 64
NS = 128
CONV = 5
SP = ("sp_0", "sp_1")
HIGHEST = lax.Precision.HIGHEST
group_eps = 1e-05
stream_eps = 1e-06


def extended(cells, sides, width):
    for axis, dim in sides:
        count = lax.axis_size(axis)
        ends = count - 1
        head = lax.slice_in_dim(cells, 0, width, axis=dim)
        tail = lax.slice_in_dim(cells, cells.shape[dim] - width, cells.shape[dim], axis=dim)
        cells = jnp.concatenate(
            [
                lax.ppermute(tail, axis, [(i, (i + 1) % count) for i in range(ends)]),
                cells,
                lax.ppermute(head, axis, [((i + 1) % count, i) for i in range(ends)]),
            ],
            axis=dim,
        )
    return cells


def filled_with(shard, identity):
    return jax.tree.map(
        lambda a, e: jnp.broadcast_to(jnp.asarray(e, a.dtype), a.shape), shard, identity
    )


def all_in_one(shard, axis):
    leaves = jax.tree.leaves(shard)
    sequence = sorted(range(len(leaves)), key=lambda k: -leaves[k].size)
    width = (1, *leaves[sequence[0]].shape)[-1]
    lines = [
        jnp.pad(leaves[k].reshape(-1), (0, -leaves[k].size % width)).reshape(-1, width)
        for k in sequence
    ]
    both, at, found = (lax.all_gather(jnp.concatenate(lines), axis), 0, {})
    for k, line in zip(sequence, lines):
        share = both[:, at : at + len(line)].reshape(len(both), -1)
        found[k] = share[:, : leaves[k].size].reshape(-1, *leaves[k].shape)
        at += len(line)
    numbers = iter(range(len(leaves)))
    return jax.tree.map(lambda _: found[next(numbers)], shard)


def carried_in(shard, axes, combine, identity, reverse):
    before = start = filled_with(shard, identity)
    so_far = shard
    for axis in reversed(axes):
        peers, mine = (lax.axis_size(axis), lax.axis_index(axis))
        pieces = all_in_one(
            jax.tree.map(
                lambda part, kind: part.astype(kind), so_far, (jnp.bfloat16, jnp.bfloat16)
            ),
            axis,
        )
        inside, so_far = (start, start)
        for k in reversed(range(peers)) if reverse else range(peers):
            passed = k > mine if reverse else k < mine
            so_far = combine(
                so_far, jax.tree.map(lambda part, own: part[k].astype(own.dtype), pieces, shard)
            )
            inside = jax.tree.map(lambda new, old: jnp.where(passed, new, old), so_far, inside)
        before = combine(inside, before)
    return before


def in_blocks(shard, dim, peers):
    shape = shard.shape
    parts = shard.reshape(*shape[:dim], peers, shape[dim] // peers, *shape[dim + 1 :])
    return jnp.moveaxis(parts, dim, 0)


def sum_at_owner(shard, axis, dim):
    peers = lax.axis_size(axis)
    parts = lax.all_to_all(in_blocks(shard, dim, peers), axis, 0, 0, tiled=True)
    return jnp.sum(parts.astype(jnp.float32), axis=0)


def block_parts(x_short, b_short, c_short, step_f, step_b, log_f, log_b):
    head_count = x_short.shape[1]
    group_count = b_short.shape[1]
    per_group = head_count // group_count
    length = x_short.shape[0]
    group_scores = jnp.einsum("tgn,sgn->gts", c_short, b_short, preferred_element_type=jnp.float32)
    x_block = x_short.astype(jnp.float32)
    b_block = b_short.astype(jnp.float32)
    c_block = c_short.astype(jnp.float32)
    scores = jnp.repeat(group_scores, per_group, axis=0)
    b_head = jnp.repeat(b_block, per_group, axis=1)
    c_head = jnp.repeat(c_block, per_group, axis=1)
    forward = jnp.cumsum(log_f, axis=1)
    backward = jnp.flip(jnp.cumsum(jnp.flip(log_b, 1), axis=1), 1)
    row_index = lax.broadcasted_iota(jnp.int32, (length, length), 0)
    col_index = lax.broadcasted_iota(jnp.int32, (length, length), 1)
    lower_mask = (col_index <= row_index)[None]
    upper_mask = (col_index >= row_index)[None]
    decay_fwd = jnp.where(
        lower_mask, jnp.exp(jnp.minimum(forward[:, :, None] - forward[:, None, :], 0.0)), 0.0
    )
    decay_bwd = jnp.where(
        upper_mask, jnp.exp(jnp.minimum(backward[:, :, None] - backward[:, None, :], 0.0)), 0.0
    )
    mixing = scores * (decay_fwd * step_f[:, None, :] + decay_bwd * step_b[:, None, :])
    within = jnp.einsum("hts,shp->thp", mixing, x_block, precision=HIGHEST)
    weight_fwd = jnp.exp(forward[:, -1:] - forward) * step_f
    weight_bwd = jnp.exp(backward[:, :1] - backward) * step_b
    state_fwd = jnp.einsum("hs,shp,shn->hpn", weight_fwd, x_block, b_head, precision=HIGHEST)
    state_bwd = jnp.einsum("hs,shp,shn->hpn", weight_bwd, x_block, b_head, precision=HIGHEST)
    return (
        within,
        state_fwd,
        state_bwd,
        forward[:, -1],
        backward[:, 0],
        jnp.exp(forward),
        jnp.exp(backward),
        c_head,
    )


def read_state(c_head, factor, state):
    return (
        jnp.einsum("thn,hpn->thp", c_head, state, precision=HIGHEST)
        * jnp.transpose(factor)[:, :, None]
    )


def compose(earlier, later):
    return (earlier[0] + later[0], earlier[1] * jnp.exp(later[0])[:, None, None] + later[1])


def body(
    skip_stream_entering,
    unfiltered_channel_feed,
    unfiltered_state_entry,
    unfiltered_state_exit,
    final_valve_preactivation,
    increment_preactivation,
    summed_attenuation_both_ways,
    channel_fading_speed,
    channel_feed_filter,
    state_entry_filter,
    state_exit_filter,
    clustered_rescale_factor,
    final_projection_weights,
    specialist_rescale_factor,
    item_specialist_couple,
    selected_cluster_likelihood,
    selected_twin_scores_raw,
    specialist_gating_weights,
    specialist_raising_weights,
    specialist_lowering_weights,
):
    tokens_here = skip_stream_entering.shape[0]
    heads_here = increment_preactivation.shape[1]
    x_width = unfiltered_channel_feed.shape[1]
    b_width = unfiltered_state_entry.shape[1]
    groups_here = b_width // NS
    joined = jnp.concatenate(
        [unfiltered_channel_feed, unfiltered_state_entry, unfiltered_state_exit], axis=1
    )
    padded = extended(joined, ((SP, 0),), CONV // 2)
    kernel = jnp.concatenate([channel_feed_filter, state_entry_filter, state_exit_filter], axis=1)
    summed = jnp.zeros(joined.shape, jnp.float32)
    for offset in range(CONV):
        summed = summed + kernel[offset] * padded[offset : offset + tokens_here].astype(jnp.float32)
    conv_out = jax.nn.silu(summed).astype(jnp.bfloat16)
    x_conv = conv_out[:, :x_width].reshape(tokens_here, heads_here, HD)
    b_conv = conv_out[:, x_width : x_width + b_width].reshape(tokens_here, groups_here, NS)
    c_conv = conv_out[:, x_width + b_width :].reshape(tokens_here, groups_here, NS)
    whole_increment_list = jax.nn.softplus(increment_preactivation)
    whole_attenuation_list = (
        -whole_increment_list * channel_fading_speed[:, :, None] + summed_attenuation_both_ways
    )
    within, state_fwd, state_bwd, total_fwd, total_bwd, factor_fwd, factor_bwd, c_head = (
        block_parts(
            x_conv,
            b_conv,
            c_conv,
            whole_increment_list[0],
            whole_increment_list[1],
            whole_attenuation_list[0],
            whole_attenuation_list[1],
        )
    )
    empty = (jnp.zeros_like(total_fwd), jnp.zeros_like(state_fwd))
    incoming_fwd = carried_in((total_fwd, state_fwd), SP, compose, empty, False)[1]
    incoming_bwd = carried_in((total_bwd, state_bwd), SP, compose, empty, True)[1]
    mixer_out = (
        within
        + read_state(c_head, factor_fwd, incoming_fwd)
        + read_state(c_head, factor_bwd, incoming_bwd)
    )
    gated = mixer_out.reshape(tokens_here, x_width) * jax.nn.silu(
        final_valve_preactivation.astype(jnp.float32)
    )
    grouped = gated.reshape(tokens_here, groups_here, -1)
    grouped = grouped * lax.rsqrt(jnp.mean(grouped * grouped, axis=-1, keepdims=True) + group_eps)
    mixed = (grouped.reshape(tokens_here, x_width) * clustered_rescale_factor).astype(jnp.bfloat16)
    projected = jnp.dot(
        lax.all_gather(mixed, "tp", axis=1, tiled=True),
        final_projection_weights,
        preferred_element_type=jnp.float32,
    )
    stream = (skip_stream_entering.astype(jnp.float32) + projected).astype(jnp.bfloat16)
    stream_f = stream.astype(jnp.float32)
    col_count = skip_stream_entering.shape[1]
    whole_rows = lax.all_gather(stream, "tp", axis=1, tiled=True).astype(jnp.float32)
    normal_rows = (
        whole_rows
        * lax.rsqrt(jnp.mean(whole_rows * whole_rows, axis=-1, keepdims=True) + stream_eps)
        * specialist_rescale_factor
    ).astype(jnp.bfloat16)
    expert_total = lax.axis_size(SP)
    capacity = 4 * tokens_here // expert_total
    flat_ids = item_specialist_couple.reshape(-1)
    assignments = flat_ids.shape[0]
    expert_iota = lax.broadcasted_iota(jnp.int32, (assignments, expert_total), 1)
    one_hot = (flat_ids[:, None] == expert_iota).astype(jnp.int32)
    ranking = jnp.sum((jnp.cumsum(one_hot, axis=0) - 1) * one_hot, axis=1)
    slot_index = flat_ids * capacity + ranking
    slot_iota = lax.broadcasted_iota(jnp.int32, (expert_total * capacity, assignments), 0)
    selector = (slot_index[None, :] == slot_iota).astype(jnp.bfloat16)
    selector = jnp.sum(selector.reshape(expert_total * capacity, tokens_here, -1), axis=2)
    weight_gate = specialist_gating_weights[0]
    weight_up = specialist_raising_weights[0]
    weight_down = specialist_lowering_weights[0]
    outgoing = jnp.dot(selector, normal_rows, preferred_element_type=jnp.float32).astype(
        jnp.bfloat16
    )
    outgoing = outgoing.reshape(expert_total, capacity, D)
    arrived = lax.all_to_all(outgoing, SP, split_axis=0, concat_axis=0, tiled=True)
    sources = arrived.shape[0]
    slot_count = arrived.shape[1]
    rows = arrived.reshape(sources * slot_count, arrived.shape[2])
    gate = jnp.dot(rows, weight_gate, preferred_element_type=jnp.float32)
    upward = jnp.dot(rows, weight_up, preferred_element_type=jnp.float32)
    hidden = (jax.nn.silu(gate) * upward).astype(jnp.bfloat16)
    partial_out = jnp.dot(hidden, weight_down, preferred_element_type=jnp.float32).astype(
        jnp.bfloat16
    )
    partial_out = partial_out.reshape(sources, slot_count, partial_out.shape[1])
    expert_cols = sum_at_owner(partial_out, "tp", 2).astype(jnp.bfloat16)
    returned = lax.all_to_all(expert_cols, SP, split_axis=0, concat_axis=0, tiled=True)
    flat_back = returned.reshape(expert_total * capacity, col_count)
    picked = (
        jnp.take(flat_back, slot_index, axis=0)
        .astype(jnp.float32)
        .reshape(tokens_here, -1, col_count)
    )
    first = jax.nn.sigmoid(selected_twin_scores_raw[:, 0] - selected_twin_scores_raw[:, 1])
    route_weight = selected_cluster_likelihood[:, None] * jnp.stack([first, 1.0 - first], axis=1)
    experts_sum = jnp.sum(route_weight[:, :, None] * picked, axis=1)
    return (stream_f + experts_sum).astype(jnp.bfloat16)


def solution(mesh):
    torus = Mesh(mesh.devices.reshape(8, 4, mesh.shape["tp"]), ("sp_0", "sp_1", "tp"))
    return jax.shard_map(
        body,
        mesh=torus,
        in_specs=(
            P(SP, "tp"),
            P(SP, "tp"),
            P(SP, "tp"),
            P(SP, "tp"),
            P(SP, "tp"),
            P(None, "tp", SP),
            P(None, "tp", SP),
            P(None, "tp"),
            P(None, "tp"),
            P(None, "tp"),
            P(None, "tp"),
            P("tp"),
            P(None, "tp"),
            P(),
            P(SP, None),
            P(SP),
            P(SP, None),
            P(SP, None, "tp"),
            P(SP, None, "tp"),
            P(SP, "tp", None),
        ),
        out_specs=P(SP, "tp"),
        check_vma=False,
    )
```

profile of v0, /device:TPU:1, one launch (start us, length us, event | category | flops | bytes accessed | tf_op | source)
XLA Modules:
  0.0 280.2 jit_solution(5651927392031734438)
XLA Ops:
  0.0 0.9 constant_dynamic-update-slice_fusion.5
  0.9 0.8 constant_dynamic-update-slice_fusion.4
  2.4 3.9 %collective-permute-start = (bf16[2,384]{1,0:T(2,128)(2,1)S(1)}, bf16[2,384]{1,0:T(2,128)(2,1)S(1)}, u32[]{:S(2)}, u32[]{:S(2)}) collective-permute-start(bf16[2,384]{1,0:T(2,128)(2,1)S(1)} %get-tuple-element.47), channel_id=1, source_target_pairs={{0,16},{16,32},{32,48},{48,64},{64,80},{80,96},{96,112},{112,128},... | collective-permute-start | bytes 4616 | tf_op jit(solution)/shard_map/ppermute | solution.py:25
  6.3 1.3 collective-permute-start.1
  7.7 0.8 copy.71
  8.8 0.8 multiply_add_fusion
  15.4 10.4 %all-gather.6 = bf16[4,129,128]{2,1,0:T(8,128)(2,1)S(1)} all-gather(bf16[1,129,128]{2,1,0:T(8,128)(2,1)S(1)} %maximum_bitcast_fusion.2), channel_id=4, replica_groups=mesh['sp_0'=8,'sp_1'=4,'tp'=16] {'sp_1'}, dimensions={0}, use_global_device_ids=true | all-gather | bytes 165120 | tf_op jit(solution)/shard_map/all_gather | solution.py:48
  26.6 27.4 %all-gather.7 = bf16[8,129,128]{2,1,0:T(8,128)(2,1)S(1)} all-gather(bf16[1,129,128]{2,1,0:T(8,128)(2,1)S(1)} %maximum_bitcast_fusion.3), channel_id=5, replica_groups=mesh['sp_0'=8,'sp_1'=4,'tp'=16] {'sp_0'}, dimensions={0}, use_global_device_ids=true | all-gather | bytes 297216 | tf_op jit(solution)/shard_map/all_gather | solution.py:48
  54.2 9.1 %all-gather.4 = bf16[4,129,128]{2,1,0:T(8,128)(2,1)S(1)} all-gather(bf16[1,129,128]{2,1,0:T(8,128)(2,1)S(1)} %maximum_bitcast_fusion), channel_id=2, replica_groups=mesh['sp_0'=8,'sp_1'=4,'tp'=16] {'sp_1'}, dimensions={0}, use_global_device_ids=true | all-gather | bytes 165120 | tf_op jit(solution)/shard_map/all_gather | solution.py:48
  64.2 18.5 %all-gather.5 = bf16[8,129,128]{2,1,0:T(8,128)(2,1)S(1)} all-gather(bf16[1,129,128]{2,1,0:T(8,128)(2,1)S(1)} %maximum_bitcast_fusion.1), channel_id=3, replica_groups=mesh['sp_0'=8,'sp_1'=4,'tp'=16] {'sp_0'}, dimensions={0}, use_global_device_ids=true | all-gather | bytes 297216 | tf_op jit(solution)/shard_map/all_gather | solution.py:48
  84.8 37.9 %all_gather.38 = bf16[128,2048]{1,0:T(8,128)(2,1)S(1)} all-gather(bf16[128,128]{1,0:T(8,128)(2,1)S(1)} %multiply_convert_fusion.1), channel_id=1, replica_groups=mesh['sp_0'=8,'sp_1'=4,'tp'=16] {'tp'}, dimensions={1}, use_global_device_ids=true | all-gather | bytes 557056 | tf_op jit(solution)/shard_map/all_gather | solution.py:213
  123.0 16.4 %all_gather.39 = bf16[128,2048]{1,0:T(8,128)(2,1)S(1)} all-gather(bf16[128,128]{1,0:T(8,128)(2,1)S(1)} %fusion.6), channel_id=1, replica_groups=mesh['sp_0'=8,'sp_1'=4,'tp'=16] {'tp'}, dimensions={1}, use_global_device_ids=true | all-gather | bytes 557056 | tf_op jit(solution)/shard_map/all_gather | solution.py:220
  139.6 0.8 convolution_convert_fusion.1
  140.4 55.6 %all_to_all.15 = bf16[32,16,2048]{2,1,0:T(8,128)(2,1)S(1)} all-to-all(bf16[32,16,2048]{2,1,0:T(8,128)(2,1)S(1)} %bitcast.252), channel_id=1, replica_groups=mesh['sp_0'=8,'sp_1'=4,'tp'=16] {'sp_0','sp_1'}, dimensions={0} | all-to-all | bytes 4194304 | tf_op jit(solution)/shard_map/all_to_all | solution.py:244
  196.0 1.5 fusion.12
  197.5 5.0 %fusion = bf16[64,8,16,128]{3,1,2,0:T(8,128)(2,1)} fusion(bf16[1,256,2048]{2,1,0:T(8,128)(2,1)S(1)} %copy-done, bf16[512,2048]{1,0:T(8,128)(2,1)S(1)} %bitcast.256, bf16[1,2048,256]{2,1,0:T(8,128)(2,1)} %param.38, f32[512,256]{1,0:T(8,128)} %fusion.12), kind=kOutput, calls=%fused_computation.4 | convolution fusion | flops 1075576832 | bytes 6815744 | tf_op jit(solution)/shard_map/dot_general | solution.py:251
  202.6 2.2 copy.83
  204.8 1.9 copy.90
  206.7 6.9 %all-to-all-start.1 = ((bf16[16,32,16,128]{3,2,1,0:T(8,128)(2,1)}), bf16[16,32,16,128]{3,2,1,0:T(8,128)(2,1)S(1)}, u32[]{:S(2)}, u32[]{:S(2)}) async-start(bf16[16,32,16,128]{3,2,1,0:T(8,128)(2,1)} %bitcast.251), calls=%async_computation.1 | async-start | bytes 4194304 | tf_op jit(solution)/shard_map/all_to_all | solution.py:87
  214.2 48.5 %all-to-all-done.1 = bf16[16,32,16,128]{3,2,1,0:T(8,128)(2,1)S(1)} async-done(((bf16[16,32,16,128]{3,2,1,0:T(8,128)(2,1)}), bf16[16,32,16,128]{3,2,1,0:T(8,128)(2,1)S(1)}, u32[]{:S(2)}, u32[]{:S(2)}) %all-to-all-start.1) | async-done | bytes 2097184 | tf_op jit(solution)/shard_map/all_to_all | solution.py:87
  262.6 0.9 reduce_sum.69
  263.6 5.3 %all-to-all-start.2 = ((bf16[32,16,128]{2,1,0:T(8,128)(2,1)}), bf16[32,16,128]{2,1,0:T(8,128)(2,1)S(1)}, u32[]{:S(2)}, u32[]{:S(2)}) async-start(bf16[32,16,128]{2,1,0:T(8,128)(2,1)} %reduce_sum.69), calls=%async_computation.2 | async-start | bytes 262144 | tf_op jit(solution)/shard_map/all_to_all | solution.py:256
  268.9 9.4 %all-to-all-done.2 = bf16[32,16,128]{2,1,0:T(8,128)(2,1)S(1)} async-done(((bf16[32,16,128]{2,1,0:T(8,128)(2,1)}), bf16[32,16,128]{2,1,0:T(8,128)(2,1)S(1)}, u32[]{:S(2)}, u32[]{:S(2)}) %all-to-all-start.2) | async-done | bytes 131104 | tf_op jit(solution)/shard_map/all_to_all | solution.py:256
  278.3 0.9 gather_fusion
  (122 shorter events, 12.6 us)
Async XLA Ops:
  0.0 197.5 %copy-start = (bf16[1,256,2048]{2,1,0:T(8,128)(2,1)S(1)}, bf16[1,256,2048]{2,1,0:T(8,128)(2,1)}, u32[]{:S(2)}) copy-start(bf16[1,256,2048]{2,1,0:T(8,128)(2,1)} %param.39) | copy-start | bytes 3145732
  2.4 12.4 %collective-permute-start = (bf16[2,384]{1,0:T(2,128)(2,1)S(1)}, bf16[2,384]{1,0:T(2,128)(2,1)S(1)}, u32[]{:S(2)}, u32[]{:S(2)}) collective-permute-start(bf16[2,384]{1,0:T(2,128)(2,1)S(1)} %get-tuple-element.47), channel_id=1, source_target_pairs={{0,16},{16,32},{32,48},{48,64},{64,80},{80,96},{96,112},{112,128},... | collective-permute-start | bytes 4616 | tf_op jit(solution)/shard_map/ppermute | solution.py:25
  6.3 8.4 %collective-permute-start.1 = (bf16[2,384]{1,0:T(2,128)(2,1)S(1)}, bf16[2,384]{1,0:T(2,128)(2,1)S(1)}, u32[]{:S(2)}, u32[]{:S(2)}) collective-permute-start(bf16[2,384]{1,0:T(2,128)(2,1)S(1)} %get-tuple-element.48), channel_id=1, source_target_pairs={{16,0},{32,16},{48,32},{64,48},{80,64},{96,80},{112,96},{128,112},... | collective-permute-start | bytes 4616 | tf_op jit(solution)/shard_map/ppermute | solution.py:27
  82.7 1.9 copy-start.2
  82.7 2.0 copy-start.7
  82.7 40.0 %copy-start.1 = (bf16[2048,128]{1,0:T(8,128)(2,1)S(1)}, bf16[2048,128]{1,0:T(8,128)(2,1)}, u32[]{:S(2)}) copy-start(bf16[2048,128]{1,0:T(8,128)(2,1)} %param.32) | copy-start | bytes 1572868
  82.7 40.0 %copy-start.3 = (bf16[128,128]{1,0:T(8,128)(2,1)S(1)}, bf16[128,128]{1,0:T(8,128)(2,1)}, u32[]{:S(2)}) copy-start(bf16[128,128]{1,0:T(8,128)(2,1)} %param.20) | copy-start | bytes 98308
  83.9 55.7 %copy-start.5 = (f32[2048]{0:T(1024)S(1)}, f32[2048]{0:T(1024)}, u32[]{:S(2)}) copy-start(f32[2048]{0:T(1024)} %param.33) | copy-start | bytes 24580
  140.4 55.6 %copy-start.9 = (bf16[1,2048,256]{2,1,0:T(8,128)(2,1)S(1)}, bf16[1,2048,256]{2,1,0:T(8,128)(2,1)}, u32[]{:S(2)}) copy-start(bf16[1,2048,256]{2,1,0:T(8,128)(2,1)} %param.37) | copy-start | bytes 3145732
  206.7 6.9 %copy-start.4 = (s32[128,2]{0,1:T(2,128)S(1)}, s32[128,2]{0,1:T(2,128)}, u32[]{:S(2)}) copy-start(s32[128,2]{0,1:T(2,128)} %param.34) | copy-start | bytes 3076
  206.7 7.3 %copy-start.6 = (f32[128,2]{0,1:T(2,128)S(1)}, f32[128,2]{0,1:T(2,128)}, u32[]{:S(2)}) copy-start(f32[128,2]{0,1:T(2,128)} %param.36) | copy-start | bytes 3076
  206.7 7.4 %copy-start.8 = (f32[128]{0:T(128)S(1)}, f32[128]{0:T(128)}, u32[]{:S(2)}) copy-start(f32[128]{0:T(128)} %param.35) | copy-start | bytes 1540
  206.7 56.0 %all-to-all-start.1 = ((bf16[16,32,16,128]{3,2,1,0:T(8,128)(2,1)}), bf16[16,32,16,128]{3,2,1,0:T(8,128)(2,1)S(1)}, u32[]{:S(2)}, u32[]{:S(2)}) async-start(bf16[16,32,16,128]{3,2,1,0:T(8,128)(2,1)} %bitcast.251), calls=%async_computation.1 | async-start | bytes 4194304 | tf_op jit(solution)/shard_map/all_to_all | solution.py:87
  263.6 14.8 %all-to-all-start.2 = ((bf16[32,16,128]{2,1,0:T(8,128)(2,1)}), bf16[32,16,128]{2,1,0:T(8,128)(2,1)S(1)}, u32[]{:S(2)}, u32[]{:S(2)}) async-start(bf16[32,16,128]{2,1,0:T(8,128)(2,1)} %reduce_sum.69), calls=%async_computation.2 | async-start | bytes 262144 | tf_op jit(solution)/shard_map/all_to_all | solution.py:256
where the time goes:
time: 281 us; the launch traced here: 280 us
  blocking collectives  175 us (62%)
  waiting for transfers between devices  57.9 us (21%)
  starting transfers between devices  17.4 us (6%)
  local copies, waits for them, and re-layouts  13.4 us (5%)
  matrix products  9.61 us (3%)
  other arithmetic  6.01 us (2%)
    all_gather x4, blocking collectives, all_in_one(): both, at, found = (lax.all_gather(jnp.concatenate(lines), axis), 0, {})  65.3 us
    all_to_all x1, blocking collectives, body(): lax.all_to_all(outgoing, SP, split_axis=0, concat_axis=0, tiled=True)  55.6 us
    all_to_all x1, waiting for transfers between devices, sum_at_owner(): parts = lax.all_to_all(in_blocks(shard, dim, peers), axis, 0, 0, tiled=True)  48.5 us
    all_gather x1, blocking collectives, body(): lax.all_gather(mixed, 'tp', axis=1, tiled=True)  37.9 us
    all_gather x1, blocking collectives, body(): lax.all_gather(stream, 'tp', axis=1, tiled=True).astype(jnp.float32)  16.4 us
    all_to_all x1, waiting for transfers between devices, body(): lax.all_to_all(expert_cols, SP, split_axis=0, concat_axis=0, tiled=True)  9.43 us
    all_to_all x1, starting transfers between devices, sum_at_owner(): parts = lax.all_to_all(in_blocks(shard, dim, peers), axis, 0, 0, tiled=True)  6.91 us
    unnamed x30, local copies, waits for them, and re-layouts  6.06 us
  transfers between devices with their start and end apart: 4, of which 2 were waited for; matrix products, arithmetic and copies ran while one was open for 3% of the time, Pallas kernels for 0%

commit v1 on v0

--- a/solution.py
+++ b/solution.py
@@ -12,6 +12,28 @@
 HIGHEST = lax.Precision.HIGHEST
 group_eps = 1e-05
 stream_eps = 1e-06
+
+
+def joined_along(pieces, dim):
+    shape = list(pieces.shape[1:])
+    shape[dim] *= pieces.shape[0]
+    return jnp.moveaxis(pieces, 0, dim).reshape(shape)
+
+
+def ring_gather(shard, axis, dim):
+    size = lax.axis_size(axis)
+    pairs = [(i, (i + 1) % size) for i in range(size)]
+    back = [(b, a) for a, b in pairs]
+    lower, upper = ([], [])
+    for lap in range(size - 1):
+        if lap % 2 == 0:
+            lower.append(lax.ppermute(lower[-1] if lower else shard, axis, pairs))
+        else:
+            upper.append(lax.ppermute(upper[-1] if upper else shard, axis, back))
+    pieces = jnp.stack([*lower[::-1], shard, *upper])
+    shift = lax.axis_index(axis) - len(lower)
+    pieces = pieces[(jnp.arange(size) - shift) % size]
+    return joined_along(pieces, dim)
 
 
 def extended(cells, sides, width):
@@ -210,9 +232,7 @@
     grouped = grouped * lax.rsqrt(jnp.mean(grouped * grouped, axis=-1, keepdims=True) + group_eps)
     mixed = (grouped.reshape(tokens_here, x_width) * clustered_rescale_factor).astype(jnp.bfloat16)
     projected = jnp.dot(
-        lax.all_gather(mixed, "tp", axis=1, tiled=True),
-        final_projection_weights,
-        preferred_element_type=jnp.float32,
+        ring_gather(mixed, "tp", 1), final_projection_weights, preferred_element_type=jnp.float32
     )
     stream = (skip_stream_entering.astype(jnp.float32) + projected).astype(jnp.bfloat16)
     stream_f = stream.astype(jnp.float32)

time: 281 us -> 299 us (1.064)
  starting transfers between devices: 17.4 us -> 63.1 us
  blocking collectives: 175 us -> 142 us
  waiting for transfers between devices: 57.9 us -> 64.3 us
    ppermute x0 -> x15, starting transfers between devices: none -> 43.8 us  [the longest x8 26.1 us: ring_gather(): lower.append(lax.ppermute(lower[-1] if lower else shard, axis, pairs))]
    all_gather x1 -> x0, blocking collectives: 37.9 us -> none  [body(): lax.all_gather(mixed, 'tp', axis=1, tiled=True)]
    ppermute x0 -> x15, waiting for transfers between devices: none -> 6.33 us  [the longest x7 4.58 us: ring_gather(): upper.append(lax.ppermute(upper[-1] if upper else shard, axis, back))]
    all_gather x1, blocking collectives: 16.4 us -> 20.2 us  [body(): lax.all_gather(stream, 'tp', axis=1, tiled=True).astype(jnp.float32)]
    unnamed x30 -> x45, local copies, waits for them, and re-layouts: 6.06 us -> 5.53 us
  transfers between devices with their start and end apart: 4 -> 19, of which waited for: 2 -> 17; matrix products, arithmetic and copies ran while one was open for 3% -> 2% of each run, Pallas kernels for 0% -> 0%
where the time goes in v1:
time: 299 us; the launch traced here: 298 us
  blocking collectives  142 us (47%)
  waiting for transfers between devices  64.3 us (22%)
  starting transfers between devices  63.1 us (21%)
  local copies, waits for them, and re-layouts  13.9 us (5%)
  matrix products  9.68 us (3%)
  other arithmetic  5.31 us (2%)
    all_gather x4, blocking collectives, all_in_one(): both, at, found = (lax.all_gather(jnp.concatenate(lines), axis), 0, {})  65.6 us
    all_to_all x1, blocking collectives, body(): lax.all_to_all(outgoing, SP, split_axis=0, concat_axis=0, tiled=True)  55.7 us
    all_to_all x1, waiting for transfers between devices, sum_at_owner(): parts = lax.all_to_all(in_blocks(shard, dim, peers), axis, 0, 0, tiled=True)  48.5 us
    ppermute x8, starting transfers between devices, ring_gather(): lower.append(lax.ppermute(lower[-1] if lower else shard, axis, pairs))  26.1 us
    all_gather x1, blocking collectives, body(): lax.all_gather(stream, 'tp', axis=1, tiled=True).astype(jnp.float32)  20.2 us
    ppermute x7, starting transfers between devices, ring_gather(): upper.append(lax.ppermute(upper[-1] if upper else shard, axis, back))  17.7 us
    all_to_all x1, waiting for transfers between devices, body(): lax.all_to_all(expert_cols, SP, split_axis=0, concat_axis=0, tiled=True)  9.43 us
    all_to_all x1, starting transfers between devices, sum_at_owner(): parts = lax.all_to_all(in_blocks(shard, dim, peers), axis, 0, 0, tiled=True)  8.68 us
  transfers between devices with their start and end apart: 19, of which 17 were waited for; matrix products, arithmetic and copies ran while one was open for 2% of the time, Pallas kernels for 0%

profile of v1, /device:TPU:1, one launch (start us, length us, event | category | flops | bytes accessed | tf_op | source)
XLA Modules:
  0.0 298.4 jit_solution(8768866199745308086)
XLA Ops:
  2.4 3.9 %collective-permute-start = (bf16[2,384]{1,0:T(2,128)(2,1)S(1)}, bf16[2,384]{1,0:T(2,128)(2,1)S(1)}, u32[]{:S(2)}, u32[]{:S(2)}) collective-permute-start(bf16[2,384]{1,0:T(2,128)(2,1)S(1)} %get-tuple-element.47), channel_id=1, source_target_pairs={{0,16},{16,32},{32,48},{48,64},{64,80},{80,96},{96,112},{112,128},... | collective-permute-start | bytes 4616 | tf_op jit(solution)/shard_map/ppermute | solution.py:47
  12.4 10.7 %all-gather.6 = bf16[4,129,128]{2,1,0:T(8,128)(2,1)S(1)} all-gather(bf16[1,129,128]{2,1,0:T(8,128)(2,1)S(1)} %maximum_bitcast_fusion.2), channel_id=4, replica_groups=mesh['sp_0'=8,'sp_1'=4,'tp'=16] {'sp_1'}, dimensions={0}, use_global_device_ids=true | all-gather | bytes 165120 | tf_op jit(solution)/shard_map/all_gather | solution.py:70
  23.9 27.0 %all-gather.7 = bf16[8,129,128]{2,1,0:T(8,128)(2,1)S(1)} all-gather(bf16[1,129,128]{2,1,0:T(8,128)(2,1)S(1)} %maximum_bitcast_fusion.3), channel_id=5, replica_groups=mesh['sp_0'=8,'sp_1'=4,'tp'=16] {'sp_0'}, dimensions={0}, use_global_device_ids=true | all-gather | bytes 297216 | tf_op jit(solution)/shard_map/all_gather | solution.py:70
  51.2 9.1 %all-gather.4 = bf16[4,129,128]{2,1,0:T(8,128)(2,1)S(1)} all-gather(bf16[1,129,128]{2,1,0:T(8,128)(2,1)S(1)} %maximum_bitcast_fusion), channel_id=2, replica_groups=mesh['sp_0'=8,'sp_1'=4,'tp'=16] {'sp_1'}, dimensions={0}, use_global_device_ids=true | all-gather | bytes 165120 | tf_op jit(solution)/shard_map/all_gather | solution.py:70
  61.2 18.8 %all-gather.5 = bf16[8,129,128]{2,1,0:T(8,128)(2,1)S(1)} all-gather(bf16[1,129,128]{2,1,0:T(8,128)(2,1)S(1)} %maximum_bitcast_fusion.1), channel_id=3, replica_groups=mesh['sp_0'=8,'sp_1'=4,'tp'=16] {'sp_0'}, dimensions={0}, use_global_device_ids=true | all-gather | bytes 297216 | tf_op jit(solution)/shard_map/all_gather | solution.py:70
  82.1 19.9 %collective-permute-start.2 = (bf16[128,128]{1,0:T(8,128)(2,1)S(1)}, bf16[128,128]{1,0:T(8,128)(2,1)S(1)}, u32[]{:S(2)}, u32[]{:S(2)}) collective-permute-start(bf16[128,128]{1,0:T(8,128)(2,1)S(1)} %multiply_convert_fusion.1), channel_id=1, source_target_pairs={{0,1},{1,2},{2,3},{3,4},{4,5},{5,6},{6,7},{7,8},{8,9},{9,10},{10,1... | collective-permute-start | bytes 98312 | tf_op jit(solution)/shard_map/ppermute | solution.py:30
  103.0 2.3 collective-permute-start.3
  106.3 2.3 collective-permute-start.4
  110.6 1.4 collective-permute-start.5
  112.8 2.2 collective-permute-start.12
  116.2 3.4 %collective-permute-start.13 = (bf16[128,128]{1,0:T(8,128)(2,1)S(1)}, bf16[128,128]{1,0:T(8,128)(2,1)S(1)}, u32[]{:S(2)}, u32[]{:S(2)}) collective-permute-start(bf16[128,128]{1,0:T(8,128)(2,1)S(1)} %collective-permute-done.12), channel_id=1, source_target_pairs={{1,0},{2,1},{3,2},{4,3},{5,4},{6,5},{7,6},{8,7},{9,8},{10,9},{11,1... | collective-permute-start | bytes 98312 | tf_op jit(solution)/shard_map/ppermute | solution.py:32
  120.5 3.7 %collective-permute-start.14 = (bf16[128,128]{1,0:T(8,128)(2,1)S(1)}, bf16[128,128]{1,0:T(8,128)(2,1)S(1)}, u32[]{:S(2)}, u32[]{:S(2)}) collective-permute-start(bf16[128,128]{1,0:T(8,128)(2,1)S(1)} %collective-permute-done.13), channel_id=1, source_target_pairs={{1,0},{2,1},{3,2},{4,3},{5,4},{6,5},{7,6},{8,7},{9,8},{10,9},{11,1... | collective-permute-start | bytes 98312 | tf_op jit(solution)/shard_map/ppermute | solution.py:32
  125.0 3.7 %collective-permute-start.15 = (bf16[128,128]{1,0:T(8,128)(2,1)S(1)}, bf16[128,128]{1,0:T(8,128)(2,1)S(1)}, u32[]{:S(2)}, u32[]{:S(2)}) collective-permute-start(bf16[128,128]{1,0:T(8,128)(2,1)S(1)} %collective-permute-done.14), channel_id=1, source_target_pairs={{1,0},{2,1},{3,2},{4,3},{5,4},{6,5},{7,6},{8,7},{9,8},{10,9},{11,1... | collective-permute-start | bytes 98312 | tf_op jit(solution)/shard_map/ppermute | solution.py:32
  129.6 3.7 %collective-permute-start.16 = (bf16[128,128]{1,0:T(8,128)(2,1)S(1)}, bf16[128,128]{1,0:T(8,128)(2,1)S(1)}, u32[]{:S(2)}, u32[]{:S(2)}) collective-permute-start(bf16[128,128]{1,0:T(8,128)(2,1)S(1)} %collective-permute-done.15), channel_id=1, source_target_pairs={{1,0},{2,1},{3,2},{4,3},{5,4},{6,5},{7,6},{8,7},{9,8},{10,9},{11,1... | collective-permute-start | bytes 98312 | tf_op jit(solution)/shard_map/ppermute | solution.py:32
  135.5 20.2 %all_gather.35 = bf16[128,2048]{1,0:T(8,128)(2,1)S(1)} all-gather(bf16[128,128]{1,0:T(8,128)(2,1)S(1)} %fusion.6), channel_id=1, replica_groups=mesh['sp_0'=8,'sp_1'=4,'tp'=16] {'tp'}, dimensions={1}, use_global_device_ids=true | all-gather | bytes 557056 | tf_op jit(solution)/shard_map/all_gather | solution.py:240
  156.7 55.7 %all_to_all.15 = bf16[32,16,2048]{2,1,0:T(8,128)(2,1)S(1)} all-to-all(bf16[32,16,2048]{2,1,0:T(8,128)(2,1)S(1)} %bitcast.288), channel_id=1, replica_groups=mesh['sp_0'=8,'sp_1'=4,'tp'=16] {'sp_0','sp_1'}, dimensions={0} | all-to-all | bytes 4194304 | tf_op jit(solution)/shard_map/all_to_all | solution.py:264
  212.4 1.5 fusion.12
  214.0 5.0 %fusion = bf16[64,8,16,128]{3,1,2,0:T(8,128)(2,1)} fusion(bf16[1,256,2048]{2,1,0:T(8,128)(2,1)S(1)} %copy-done, bf16[512,2048]{1,0:T(8,128)(2,1)S(1)} %bitcast.292, bf16[1,2048,256]{2,1,0:T(8,128)(2,1)} %param.38, f32[512,256]{1,0:T(8,128)} %fusion.12), kind=kOutput, calls=%fused_computation.5 | convolution fusion | flops 1075576832 | bytes 6815744 | tf_op jit(solution)/shard_map/dot_general | solution.py:271
  219.0 2.2 copy.87
  221.2 1.9 copy.94
  223.1 8.7 %all-to-all-start.1 = ((bf16[16,32,16,128]{3,2,1,0:T(8,128)(2,1)}), bf16[16,32,16,128]{3,2,1,0:T(8,128)(2,1)S(1)}, u32[]{:S(2)}, u32[]{:S(2)}) async-start(bf16[16,32,16,128]{3,2,1,0:T(8,128)(2,1)} %bitcast.287), calls=%async_computation.1 | async-start | bytes 4194304 | tf_op jit(solution)/shard_map/all_to_all | solution.py:109
  232.3 48.5 %all-to-all-done.1 = bf16[16,32,16,128]{3,2,1,0:T(8,128)(2,1)S(1)} async-done(((bf16[16,32,16,128]{3,2,1,0:T(8,128)(2,1)}), bf16[16,32,16,128]{3,2,1,0:T(8,128)(2,1)S(1)}, u32[]{:S(2)}, u32[]{:S(2)}) %all-to-all-start.1) | async-done | bytes 2097184 | tf_op jit(solution)/shard_map/all_to_all | solution.py:109
  281.8 5.3 %all-to-all-start.2 = ((bf16[32,16,128]{2,1,0:T(8,128)(2,1)}), bf16[32,16,128]{2,1,0:T(8,128)(2,1)S(1)}, u32[]{:S(2)}, u32[]{:S(2)}) async-start(bf16[32,16,128]{2,1,0:T(8,128)(2,1)} %reduce_sum.69), calls=%async_computation.2 | async-start | bytes 262144 | tf_op jit(solution)/shard_map/all_to_all | solution.py:276
  287.1 9.4 %all-to-all-done.2 = bf16[32,16,128]{2,1,0:T(8,128)(2,1)S(1)} async-done(((bf16[32,16,128]{2,1,0:T(8,128)(2,1)}), bf16[32,16,128]{2,1,0:T(8,128)(2,1)S(1)}, u32[]{:S(2)}, u32[]{:S(2)}) %all-to-all-start.2) | async-done | bytes 131104 | tf_op jit(solution)/shard_map/all_to_all | solution.py:276
  (171 shorter events, 27.1 us)
Async XLA Ops:
  0.0 214.0 %copy-start = (bf16[1,256,2048]{2,1,0:T(8,128)(2,1)S(1)}, bf16[1,256,2048]{2,1,0:T(8,128)(2,1)}, u32[]{:S(2)}) copy-start(bf16[1,256,2048]{2,1,0:T(8,128)(2,1)} %param.39) | copy-start | bytes 3145732
  2.4 9.4 %collective-permute-start = (bf16[2,384]{1,0:T(2,128)(2,1)S(1)}, bf16[2,384]{1,0:T(2,128)(2,1)S(1)}, u32[]{:S(2)}, u32[]{:S(2)}) collective-permute-start(bf16[2,384]{1,0:T(2,128)(2,1)S(1)} %get-tuple-element.47), channel_id=1, source_target_pairs={{0,16},{16,32},{32,48},{48,64},{64,80},{80,96},{96,112},{112,128},... | collective-permute-start | bytes 4616 | tf_op jit(solution)/shard_map/ppermute | solution.py:47
  6.3 5.5 %collective-permute-start.1 = (bf16[2,384]{1,0:T(2,128)(2,1)S(1)}, bf16[2,384]{1,0:T(2,128)(2,1)S(1)}, u32[]{:S(2)}, u32[]{:S(2)}) collective-permute-start(bf16[2,384]{1,0:T(2,128)(2,1)S(1)} %get-tuple-element.48), channel_id=1, source_target_pairs={{16,0},{32,16},{48,32},{64,48},{80,64},{96,80},{112,96},{128,112},... | collective-permute-start | bytes 4616 | tf_op jit(solution)/shard_map/ppermute | solution.py:49
  80.0 22.0 %copy-start.4 = (s32[128,2]{0,1:T(2,128)S(1)}, s32[128,2]{0,1:T(2,128)}, u32[]{:S(2)}) copy-start(s32[128,2]{0,1:T(2,128)} %param.34) | copy-start | bytes 3076
  81.7 53.4 %copy-start.1 = (bf16[2048,128]{1,0:T(8,128)(2,1)S(1)}, bf16[2048,128]{1,0:T(8,128)(2,1)}, u32[]{:S(2)}) copy-start(bf16[2048,128]{1,0:T(8,128)(2,1)} %param.32) | copy-start | bytes 1572868
  81.7 53.4 %copy-start.3 = (bf16[128,128]{1,0:T(8,128)(2,1)S(1)}, bf16[128,128]{1,0:T(8,128)(2,1)}, u32[]{:S(2)}) copy-start(bf16[128,128]{1,0:T(8,128)(2,1)} %param.20) | copy-start | bytes 98308
  82.1 20.9 %collective-permute-start.2 = (bf16[128,128]{1,0:T(8,128)(2,1)S(1)}, bf16[128,128]{1,0:T(8,128)(2,1)S(1)}, u32[]{:S(2)}, u32[]{:S(2)}) collective-permute-start(bf16[128,128]{1,0:T(8,128)(2,1)S(1)} %multiply_convert_fusion.1), channel_id=1, source_target_pairs={{0,1},{1,2},{2,3},{3,4},{4,5},{5,6},{6,7},{7,8},{8,9},{9,10},{10,1... | collective-permute-start | bytes 98312 | tf_op jit(solution)/shard_map/ppermute | solution.py:30
  103.0 3.3 %collective-permute-start.3 = (bf16[128,128]{1,0:T(8,128)(2,1)S(1)}, bf16[128,128]{1,0:T(8,128)(2,1)S(1)}, u32[]{:S(2)}, u32[]{:S(2)}) collective-permute-start(bf16[128,128]{1,0:T(8,128)(2,1)S(1)} %collective-permute-done.2), channel_id=1, source_target_pairs={{0,1},{1,2},{2,3},{3,4},{4,5},{5,6},{6,7},{7,8},{8,9},{9,10},{10,1... | collective-permute-start | bytes 98312 | tf_op jit(solution)/shard_map/ppermute | solution.py:30
  105.9 3.6 %collective-permute-start.10 = (bf16[128,128]{1,0:T(8,128)(2,1)S(1)}, bf16[128,128]{1,0:T(8,128)(2,1)S(1)}, u32[]{:S(2)}, u32[]{:S(2)}) collective-permute-start(bf16[128,128]{1,0:T(8,128)(2,1)S(1)} %multiply_convert_fusion.1), channel_id=1, source_target_pairs={{1,0},{2,1},{3,2},{4,3},{5,4},{6,5},{7,6},{8,7},{9,8},{10,9},{11,1... | collective-permute-start | bytes 98312 | tf_op jit(solution)/shard_map/ppermute | solution.py:32
  106.3 4.3 %collective-permute-start.4 = (bf16[128,128]{1,0:T(8,128)(2,1)S(1)}, bf16[128,128]{1,0:T(8,128)(2,1)S(1)}, u32[]{:S(2)}, u32[]{:S(2)}) collective-permute-start(bf16[128,128]{1,0:T(8,128)(2,1)S(1)} %collective-permute-done.3), channel_id=1, source_target_pairs={{0,1},{1,2},{2,3},{3,4},{4,5},{5,6},{6,7},{7,8},{8,9},{9,10},{10,1... | collective-permute-start | bytes 98312 | tf_op jit(solution)/shard_map/ppermute | solution.py:30
  109.5 3.3 %collective-permute-start.11 = (bf16[128,128]{1,0:T(8,128)(2,1)S(1)}, bf16[128,128]{1,0:T(8,128)(2,1)S(1)}, u32[]{:S(2)}, u32[]{:S(2)}) collective-permute-start(bf16[128,128]{1,0:T(8,128)(2,1)S(1)} %collective-permute-done.10), channel_id=1, source_target_pairs={{1,0},{2,1},{3,2},{4,3},{5,4},{6,5},{7,6},{8,7},{9,8},{10,9},{11,1... | collective-permute-start | bytes 98312 | tf_op jit(solution)/shard_map/ppermute | solution.py:32
  110.6 4.6 %collective-permute-start.5 = (bf16[128,128]{1,0:T(8,128)(2,1)S(1)}, bf16[128,128]{1,0:T(8,128)(2,1)S(1)}, u32[]{:S(2)}, u32[]{:S(2)}) collective-permute-start(bf16[128,128]{1,0:T(8,128)(2,1)S(1)} %collective-permute-done.4), channel_id=1, source_target_pairs={{0,1},{1,2},{2,3},{3,4},{4,5},{5,6},{6,7},{7,8},{8,9},{9,10},{10,1... | collective-permute-start | bytes 98312 | tf_op jit(solution)/shard_map/ppermute | solution.py:30
  112.8 3.3 %collective-permute-start.12 = (bf16[128,128]{1,0:T(8,128)(2,1)S(1)}, bf16[128,128]{1,0:T(8,128)(2,1)S(1)}, u32[]{:S(2)}, u32[]{:S(2)}) collective-permute-start(bf16[128,128]{1,0:T(8,128)(2,1)S(1)} %collective-permute-done.11), channel_id=1, source_target_pairs={{1,0},{2,1},{3,2},{4,3},{5,4},{6,5},{7,6},{8,7},{9,8},{10,9},{11,1... | collective-permute-start | bytes 98312 | tf_op jit(solution)/shard_map/ppermute | solution.py:32
  115.1 4.6 %collective-permute-start.6 = (bf16[128,128]{1,0:T(8,128)(2,1)S(1)}, bf16[128,128]{1,0:T(8,128)(2,1)S(1)}, u32[]{:S(2)}, u32[]{:S(2)}) collective-permute-start(bf16[128,128]{1,0:T(8,128)(2,1)S(1)} %collective-permute-done.5), channel_id=1, source_target_pairs={{0,1},{1,2},{2,3},{3,4},{4,5},{5,6},{6,7},{7,8},{8,9},{9,10},{10,1... | collective-permute-start | bytes 98312 | tf_op jit(solution)/shard_map/ppermute | solution.py:30
  116.2 4.3 %collective-permute-start.13 = (bf16[128,128]{1,0:T(8,128)(2,1)S(1)}, bf16[128,128]{1,0:T(8,128)(2,1)S(1)}, u32[]{:S(2)}, u32[]{:S(2)}) collective-permute-start(bf16[128,128]{1,0:T(8,128)(2,1)S(1)} %collective-permute-done.12), channel_id=1, source_target_pairs={{1,0},{2,1},{3,2},{4,3},{5,4},{6,5},{7,6},{8,7},{9,8},{10,9},{11,1... | collective-permute-start | bytes 98312 | tf_op jit(solution)/shard_map/ppermute | solution.py:32
  119.7 4.6 %collective-permute-start.7 = (bf16[128,128]{1,0:T(8,128)(2,1)S(1)}, bf16[128,128]{1,0:T(8,128)(2,1)S(1)}, u32[]{:S(2)}, u32[]{:S(2)}) collective-permute-start(bf16[128,128]{1,0:T(8,128)(2,1)S(1)} %collective-permute-done.6), channel_id=1, source_target_pairs={{0,1},{1,2},{2,3},{3,4},{4,5},{5,6},{6,7},{7,8},{8,9},{9,10},{10,1... | collective-permute-start | bytes 98312 | tf_op jit(solution)/shard_map/ppermute | solution.py:30
  120.5 4.6 %collective-permute-start.14 = (bf16[128,128]{1,0:T(8,128)(2,1)S(1)}, bf16[128,128]{1,0:T(8,128)(2,1)S(1)}, u32[]{:S(2)}, u32[]{:S(2)}) collective-permute-start(bf16[128,128]{1,0:T(8,128)(2,1)S(1)} %collective-permute-done.13), channel_id=1, source_target_pairs={{1,0},{2,1},{3,2},{4,3},{5,4},{6,5},{7,6},{8,7},{9,8},{10,9},{11,1... | collective-permute-start | bytes 98312 | tf_op jit(solution)/shard_map/ppermute | solution.py:32
  124.2 4.6 %collective-permute-start.8 = (bf16[128,128]{1,0:T(8,128)(2,1)S(1)}, bf16[128,128]{1,0:T(8,128)(2,1)S(1)}, u32[]{:S(2)}, u32[]{:S(2)}) collective-permute-start(bf16[128,128]{1,0:T(8,128)(2,1)S(1)} %collective-permute-done.7), channel_id=1, source_target_pairs={{0,1},{1,2},{2,3},{3,4},{4,5},{5,6},{6,7},{7,8},{8,9},{9,10},{10,1... | collective-permute-start | bytes 98312 | tf_op jit(solution)/shard_map/ppermute | solution.py:30
  125.0 4.6 %collective-permute-start.15 = (bf16[128,128]{1,0:T(8,128)(2,1)S(1)}, bf16[128,128]{1,0:T(8,128)(2,1)S(1)}, u32[]{:S(2)}, u32[]{:S(2)}) collective-permute-start(bf16[128,128]{1,0:T(8,128)(2,1)S(1)} %collective-permute-done.14), channel_id=1, source_target_pairs={{1,0},{2,1},{3,2},{4,3},{5,4},{6,5},{7,6},{8,7},{9,8},{10,9},{11,1... | collective-permute-start | bytes 98312 | tf_op jit(solution)/shard_map/ppermute | solution.py:32
  128.8 4.6 %collective-permute-start.9 = (bf16[128,128]{1,0:T(8,128)(2,1)S(1)}, bf16[128,128]{1,0:T(8,128)(2,1)S(1)}, u32[]{:S(2)}, u32[]{:S(2)}) collective-permute-start(bf16[128,128]{1,0:T(8,128)(2,1)S(1)} %collective-permute-done.8), channel_id=1, source_target_pairs={{0,1},{1,2},{2,3},{3,4},{4,5},{5,6},{6,7},{7,8},{8,9},{9,10},{10,1... | collective-permute-start | bytes 98312 | tf_op jit(solution)/shard_map/ppermute | solution.py:30
  129.6 4.6 %collective-permute-start.16 = (bf16[128,128]{1,0:T(8,128)(2,1)S(1)}, bf16[128,128]{1,0:T(8,128)(2,1)S(1)}, u32[]{:S(2)}, u32[]{:S(2)}) collective-permute-start(bf16[128,128]{1,0:T(8,128)(2,1)S(1)} %collective-permute-done.15), channel_id=1, source_target_pairs={{1,0},{2,1},{3,2},{4,3},{5,4},{6,5},{7,6},{8,7},{9,8},{10,9},{11,1... | collective-permute-start | bytes 98312 | tf_op jit(solution)/shard_map/ppermute | solution.py:32
  156.7 55.7 %copy-start.9 = (bf16[1,2048,256]{2,1,0:T(8,128)(2,1)S(1)}, bf16[1,2048,256]{2,1,0:T(8,128)(2,1)}, u32[]{:S(2)}) copy-start(bf16[1,2048,256]{2,1,0:T(8,128)(2,1)} %param.37) | copy-start | bytes 3145732
  223.1 57.7 %all-to-all-start.1 = ((bf16[16,32,16,128]{3,2,1,0:T(8,128)(2,1)}), bf16[16,32,16,128]{3,2,1,0:T(8,128)(2,1)S(1)}, u32[]{:S(2)}, u32[]{:S(2)}) async-start(bf16[16,32,16,128]{3,2,1,0:T(8,128)(2,1)} %bitcast.287), calls=%async_computation.1 | async-start | bytes 4194304 | tf_op jit(solution)/shard_map/all_to_all | solution.py:109
  281.8 14.8 %all-to-all-start.2 = ((bf16[32,16,128]{2,1,0:T(8,128)(2,1)}), bf16[32,16,128]{2,1,0:T(8,128)(2,1)S(1)}, u32[]{:S(2)}, u32[]{:S(2)}) async-start(bf16[32,16,128]{2,1,0:T(8,128)(2,1)} %reduce_sum.69), calls=%async_computation.2 | async-start | bytes 262144 | tf_op jit(solution)/shard_map/all_to_all | solution.py:276
  (5 other events, 43.9 us)
